TPU v7x, 256 devices: a 4x2x16 block of a 4x16x16 slice. The times are simulated.
256 devices in a mesh: grp: 2 (over y), fs: 32 (over z, core), tp: 4 (over x).
Axes of the slice: x: 4, y: 2, z: 16, core: 2. Of those that a mesh axis runs over, the one named last changes fastest.
The devices are a block of a 4x16x16 slice.
Arguments:
- prompt: bfloat16 [24576, 2048], P(('grp', 'fs')), parts along dimension 0, may hold values from -6 to 6
- routes: int32 [24576, 4], P(('grp', 'fs')), parts along dimension 0, may hold values from 0 to 31, all different within a row; in each aligned block of 384 rows (0 to 383, 384 to 767, ...) at most 60 rows name the same one
- route_weight: float32 [24576, 4], P(('grp', 'fs')), parts along dimension 0, may hold values from 0.2 to 1
- norm_gain: float32 [2048], P('fs'), may hold values from 0.1 to 1.9
- gate_train: float32 [32, 2048, 1024], P(None, 'fs', 'tp'), may hold values from -0.4 to 0.4
- up_train: float32 [32, 2048, 1024], P(None, 'fs', 'tp'), may hold values from -0.4 to 0.4
- down_train: float32 [32, 1024, 2048], P(None, 'fs', 'tp'), may hold values from -0.07 to 0.07
Outputs:
- gate_serve: bfloat16 [64, 2048, 1024], P(('grp', 'fs'), None, 'tp'), parts along dimension 0
- up_serve: bfloat16 [64, 2048, 1024], P(('grp', 'fs'), None, 'tp'), parts along dimension 0
- down_serve: bfloat16 [64, 1024, 2048], P(('grp', 'fs'), 'tp'), parts along dimension 0
- mixed: bfloat16 [24576, 2048], P(('grp', 'fs'), 'tp'), parts along dimension 0
There are 2 independent parts, one for each index of `grp`. A program takes and returns all parts, laid end to end along the dimension named above; an argument that names none is the same for every part. Nothing has to cross between parts.
Inputs may be any that keep to these rules, and one draw needn't show every extreme that they name: `routes`: each row names 4 different experts. Among the rows of one index of fs no expert is named more than 60 times, a bound that some block reaches on some index.
All inputs are finite; a program needn't handle non-finite values.
Results may differ from a plain program's by a relative error of at most 0.012.
Values may be sent and summed in bfloat16 or wider, within the bound.
A program may use at most 128 MiB of HBM per device.

v0:
```python
import jax
import jax.numpy as jnp
from jax import lax
from jax.sharding import Mesh
from jax.sharding import PartitionSpec as P

LIMIT = 7.0
ALPHA = 1.702
EPS = 1e-06
FS = ("z", "core")
ROWS = ("gh", "gl", "z", "core")


def shards(prompt, routes, route_weight, norm_gain, gate_train, up_train, down_train):
    bf16, f32 = jnp.bfloat16, jnp.float32
    n_tp = lax.axis_size("tp")
    k = lax.axis_index("tp")
    experts, gate_rows, ff = gate_train.shape
    down_rows, cols = down_train.shape[1:]
    gate = (norm_gain[None, :, None] * gate_train).astype(bf16)
    up = (norm_gain[None, :, None] * up_train).astype(bf16)
    both = jnp.concatenate((gate, up), axis=2)
    w = jnp.concatenate((both, down_train.astype(bf16)), axis=1)
    half = w.shape[1] // 2
    mine = lax.dynamic_slice_in_dim(w, lax.axis_index("gl") * half, half, 1)
    mine = lax.all_to_all(mine, FS, split_axis=0, concat_axis=0, tiled=True)
    wk = lax.all_gather(mine, "gl", axis=1, tiled=True)
    wf = lax.all_gather(wk, "tp", axis=0)
    tok = prompt.shape[0] // n_tp
    x = lax.dynamic_slice_in_dim(prompt, k * tok, tok, 0).astype(f32)
    x = (x * lax.rsqrt(jnp.mean(x * x, axis=-1, keepdims=True) + EPS)).astype(bf16)
    r = lax.dynamic_slice_in_dim(routes, k * tok, tok, 0)
    rw = lax.dynamic_slice_in_dim(route_weight, k * tok, tok, 0)
    hot = r[:, :, None] == jnp.arange(experts, dtype=jnp.int32)[None, None, :]
    c = jnp.sum(jnp.where(hot, rw[:, :, None], 0.0), axis=1).T
    xt = lax.all_gather(x, FS, axis=0)
    call = lax.all_to_all(c, FS, split_axis=0, concat_axis=0, tiled=True)
    n_fs = xt.shape[0]
    d = xt.shape[2]
    flat = xt.reshape(n_fs * tok, d)
    out_cols = []
    hid = []
    for t in range(n_tp):
        g = jnp.dot(flat, wf[t, :, :gate_rows, :ff].reshape(d, ff), preferred_element_type=f32)
        u = jnp.dot(flat, wf[t, :, :gate_rows, ff:].reshape(d, ff), preferred_element_type=f32)
        g = jnp.minimum(g, LIMIT)
        u = jnp.clip(u, -LIMIT, LIMIT)
        hid.append(((u + 1.0) * g * jax.nn.sigmoid(ALPHA * g)).astype(bf16))
    hidden = jnp.concatenate(hid, axis=1)
    scale = call.reshape(n_fs * tok, 1)
    for t in range(n_tp):
        down = wf[t, :, gate_rows:, :].reshape(n_fs * down_rows, cols)
        out_cols.append((scale * jnp.dot(hidden, down, preferred_element_type=f32)).astype(bf16))
    out = jnp.concatenate(out_cols, axis=1)
    summed = lax.psum_scatter(out, FS, scatter_dimension=0, tiled=True)
    mixed = lax.all_to_all(summed, "tp", split_axis=1, concat_axis=0, tiled=True)
    own = wk[:, :gate_rows].reshape(1, d, 2 * ff)
    share = n_fs // n_tp
    down_own = lax.dynamic_slice_in_dim(wf, k * share, share, 1)[:, :, gate_rows:, :]
    down_own = jnp.moveaxis(down_own.reshape(n_tp, share * down_rows, cols), 0, 1).reshape(1, share * down_rows, n_tp * cols)
    return (own[:, :, :ff], own[:, :, ff:], down_own, mixed)


def solution(mesh):
    groups, n_tp = mesh.shape["grp"], mesh.shape["tp"]
    chips = mesh.shape["fs"] // 2
    pair = 2 if groups % 2 == 0 else 1
    finer = Mesh(
        mesh.devices.reshape(groups // pair, pair, chips, 2, n_tp),
        ("gh", "gl", "z", "core", "tp"),
    )
    return jax.shard_map(
        shards,
        mesh=finer,
        in_specs=(P(ROWS), P(ROWS), P(ROWS), P(FS), P(None, FS, "tp"), P(None, FS, "tp"), P(None, FS, "tp")),
        out_specs=(P(ROWS, None, "tp"), P(ROWS, None, "tp"), P(ROWS, "tp", None), P(ROWS, "tp")),
        check_vma=False,
    )
```

profile of v0, /device:TPU:40, one launch (start us, length us, event | category | flops | bytes accessed | tf_op | source)
XLA Modules:
  0.0 652.7 jit_solution(17831976317860119267)
XLA Ops:
  9.4 2.3 multiply_convert_fusion.4
  12.4 102.8 %all_to_all.33 = bf16[32,48,512]{2,1,0:T(8,128)(2,1)} all-to-all(bf16[32,48,512]{2,1,0:T(8,128)(2,1)S(1)} %fusion.17), channel_id=1, replica_groups=mesh['gh'=1,'gl'=2,'z'=16,'core'=2,'tp'=4] {'z','core'}, dimensions={0} | all-to-all | bytes 3145728 | tf_op jit(solution)/shard_map/all_to_all | solution.py:26
  115.3 44.2 %all-gather.6.cloned.1.call-done = bf16[32,96,512]{2,1,0:T(8,128)(2,1)} async-done(((bf16[32,48,512]{2,1,0:T(8,128)(2,1)}), bf16[32,96,512]{2,1,0:T(8,128)(2,1)}) %all-gather.6.cloned.1.call-update) | async-done | bytes 3145744 | tf_op jit(solution)/shard_map/all_gather | solution.py:27
  161.8 24.9 %all_to_all.34 = f32[32,1,96]{2,1,0:T(1,128)S(1)} all-to-all(f32[32,1,96]{2,1,0:T(1,128)S(1)} %bitcast.68), channel_id=1, replica_groups=mesh['gh'=1,'gl'=2,'z'=16,'core'=2,'tp'=4] {'z','core'}, dimensions={0} | all-to-all | bytes 24576 | tf_op jit(solution)/shard_map/all_to_all | solution.py:37
  188.0 99.6 %all-gather.8.cloned.1.call-done = bf16[128,96,512]{2,1,0:T(8,128)(2,1)} async-done(((bf16[32,96,512]{2,1,0:T(8,128)(2,1)}), bf16[128,96,512]{2,1,0:T(8,128)(2,1)}) %all-gather.8.cloned.1.call-update) | async-done | bytes 12582928 | tf_op jit(solution)/shard_map/all_gather | solution.py:28
  287.5 4.4 fusion.20
  292.0 6.1 fusion.21
  298.0 78.2 %all-gather.10.cloned.1.call-done = bf16[3072,2048]{1,0:T(8,128)(2,1)} async-done(((bf16[96,2048]{1,0:T(8,128)(2,1)}), bf16[3072,2048]{1,0:T(8,128)(2,1)}) %all-gather.10.cloned.1.call-update) | async-done | bytes 12582928 | tf_op jit(solution)/shard_map/all_gather | solution.py:36
  376.3 10.1 %convolution_minimum_fusion.2 = f32[3072,256]{0,1:T(8,128)} fusion(bf16[3072,2048]{1,0:T(8,128)(2,1)} %all-gather.10.cloned.1.call-done, bf16[2048,256]{1,0:T(8,128)(2,1)} %bitcast.63), kind=kOutput, calls=%fused_computation.8 | convolution fusion | flops 3222011904 | bytes 16777216 | tf_op jit(solution)/shard_map/dot_general | solution.py:44
  386.3 9.9 %convolution_minimum_fusion.3 = f32[3072,256]{0,1:T(8,128)} fusion(bf16[3072,2048]{1,0:T(8,128)(2,1)} %all-gather.10.cloned.1.call-done, bf16[2048,256]{1,0:T(8,128)(2,1)S(1)} %bitcast.62), kind=kOutput, calls=%fused_computation.9 | convolution fusion | flops 3222011904 | bytes 16777216 | tf_op jit(solution)/shard_map/dot_general | solution.py:44
  396.2 9.9 %convolution_minimum_fusion.1 = f32[3072,256]{0,1:T(8,128)} fusion(bf16[3072,2048]{1,0:T(8,128)(2,1)} %all-gather.10.cloned.1.call-done, bf16[2048,256]{1,0:T(8,128)(2,1)S(1)} %bitcast.61), kind=kOutput, calls=%fused_computation.7 | convolution fusion | flops 3222011904 | bytes 16777216 | tf_op jit(solution)/shard_map/dot_general | solution.py:44
  406.1 10.0 %convolution_minimum_fusion = f32[3072,256]{0,1:T(8,128)} fusion(bf16[3072,2048]{1,0:T(8,128)(2,1)} %all-gather.10.cloned.1.call-done, bf16[2048,256]{1,0:T(8,128)(2,1)S(1)} %bitcast.60), kind=kOutput, calls=%fused_computation.6 | convolution fusion | flops 3222011904 | bytes 16777216 | tf_op jit(solution)/shard_map/dot_general | solution.py:44
  416.1 15.0 %fusion.11 = bf16[3072,256]{0,1:T(8,128)(2,1)} fusion(f32[3072,256]{0,1:T(8,128)} %convolution_minimum_fusion.2, bf16[3072,2048]{1,0:T(8,128)(2,1)} %all-gather.10.cloned.1.call-done, bf16[2048,256]{1,0:T(8,128)(2,1)S(1)} %bitcast.59), kind=kOutput, calls=%fused_computation.24 | convolution fusion | flops 3228303360 | bytes 18350080 | tf_op jit(solution)/shard_map/dot_general | solution.py:45
  431.1 10.1 %fusion.15 = bf16[3072,256]{0,1:T(8,128)(2,1)} fusion(f32[3072,256]{0,1:T(8,128)S(1)} %copy-done.16, bf16[3072,2048]{1,0:T(8,128)(2,1)} %all-gather.10.cloned.1.call-done, bf16[2048,256]{1,0:T(8,128)(2,1)S(1)} %bitcast.58), kind=kOutput, calls=%fused_computation.29 | convolution fusion | flops 3228303360 | bytes 18350080 | tf_op jit(solution)/shard_map/dot_general | solution.py:45
  441.2 15.4 %fusion.7 = bf16[3072,256]{0,1:T(8,128)(2,1)} fusion(f32[3072,256]{0,1:T(8,128)} %convolution_minimum_fusion.1, bf16[3072,2048]{1,0:T(8,128)(2,1)} %all-gather.10.cloned.1.call-done, bf16[2048,256]{1,0:T(8,128)(2,1)S(1)} %bitcast.57), kind=kOutput, calls=%fused_computation.19 | convolution fusion | flops 3228303360 | bytes 18350080 | tf_op jit(solution)/shard_map/dot_general | solution.py:45
  456.6 10.3 %fusion.3 = bf16[3072,256]{0,1:T(8,128)(2,1)} fusion(f32[3072,256]{0,1:T(8,128)S(1)} %copy-done.15, bf16[3072,2048]{1,0:T(8,128)(2,1)} %all-gather.10.cloned.1.call-done, bf16[2048,256]{1,0:T(8,128)(2,1)S(1)} %bitcast.56), kind=kOutput, calls=%fused_computation.14 | convolution fusion | flops 3228303360 | bytes 18350080 | tf_op jit(solution)/shard_map/dot_general | solution.py:45
  467.0 5.5 multiply_convert_fusion.3
  472.5 4.4 multiply_convert_fusion.2
  476.9 4.3 multiply_convert_fusion.1
  481.3 4.5 multiply_convert_fusion
  485.8 5.8 pad_maximum_fusion
  491.6 15.7 %copy.26 = bf16[3072,2048]{1,0:T(8,128)(2,1)} copy(bf16[3072,2048]{0,1:T(8,128)(2,1)} %pad_maximum_fusion) | data formatting | bytes 25165824
  510.7 120.6 %reduce-scatter.4.cloned.1.call-done = bf16[96,2048]{1,0:T(8,128)(2,1)} async-done(((bf16[3072,2048]{1,0:T(8,128)(2,1)}), bf16[96,2048]{1,0:T(8,128)(2,1)}) %reduce-scatter.4.cloned.1.call-update) | async-done | bytes 393232
  633.6 4.3 all-to-all-start.2
  (70 shorter events, 20.3 us)
Async XLA Ops:
  7.2 153.7 %copy-start = (f32[384,4]{0,1:T(4,128)S(1)}, f32[384,4]{0,1:T(4,128)}, u32[]{:S(2)}) copy-start(f32[384,4]{0,1:T(4,128)} %param.9) | copy-start | bytes 18436
  7.2 2.2 copy-start.4
  7.2 152.3 %all-gather.6.cloned.1.call-start = ((), (), s32[]{:S(2)}) async-start(), calls=%async_computation.4 | async-start | bytes 4718592 | tf_op jit(solution)/shard_map/all_gather | solution.py:27
  115.2 44.5 %copy-start.13 = (bf16[384,2048]{1,0:T(8,128)(2,1)S(1)}, bf16[384,2048]{1,0:T(8,128)(2,1)}, u32[]{:S(2)}) copy-start(bf16[384,2048]{1,0:T(8,128)(2,1)} %param.7) | copy-start | bytes 4718596
  115.3 172.3 %all-gather.8.cloned.1.call-start = ((), (), s32[]{:S(2)}) async-start(), calls=%async_computation.5 | async-start | bytes 15728640 | tf_op jit(solution)/shard_map/all_gather | solution.py:28
  159.6 216.7 %all-gather.10.cloned.1.call-start = ((), (), s32[]{:S(2)}) async-start(), calls=%async_computation.6 | async-start | bytes 12976128 | tf_op jit(solution)/shard_map/all_gather | solution.py:36
  160.8 470.5 %reduce-scatter.4.cloned.1.call-start = ((), (), s32[]{:S(2)}) async-start(), calls=%async_computation.7 | async-start | bytes 12976128
  376.3 10.1 %copy-start.8 = (bf16[1,32,64,256]{3,2,1,0:T(8,128)(2,1)S(1)}, bf16[1,32,64,256]{3,2,1,0:T(8,128)(2,1)}, u32[]{:S(2)}) copy-start(bf16[1,32,64,256]{3,2,1,0:T(8,128)(2,1)} %get-tuple-element.15) | copy-start | bytes 3145732
  386.3 9.9 %copy-start.7 = (bf16[1,32,64,256]{3,2,1,0:T(8,128)(2,1)S(1)}, bf16[1,32,64,256]{3,2,1,0:T(8,128)(2,1)}, u32[]{:S(2)}) copy-start(bf16[1,32,64,256]{3,2,1,0:T(8,128)(2,1)} %get-tuple-element.11) | copy-start | bytes 3145732
  396.2 9.9 %copy-start.6 = (bf16[1,32,64,256]{3,2,1,0:T(8,128)(2,1)S(1)}, bf16[1,32,64,256]{3,2,1,0:T(8,128)(2,1)}, u32[]{:S(2)}) copy-start(bf16[1,32,64,256]{3,2,1,0:T(8,128)(2,1)} %get-tuple-element.9) | copy-start | bytes 3145732
  406.1 10.0 %copy-start.5 = (bf16[1,32,64,256]{3,2,1,0:T(8,128)(2,1)S(1)}, bf16[1,32,64,256]{3,2,1,0:T(8,128)(2,1)}, u32[]{:S(2)}) copy-start(bf16[1,32,64,256]{3,2,1,0:T(8,128)(2,1)} %get-tuple-element.14) | copy-start | bytes 3145732
  416.1 15.0 %copy-start.16 = (f32[3072,256]{0,1:T(8,128)S(1)}, f32[3072,256]{0,1:T(8,128)}, u32[]{:S(2)}) copy-start(f32[3072,256]{0,1:T(8,128)} %convolution_minimum_fusion.3) | copy-start | bytes 9437188
  441.2 15.4 %copy-start.15 = (f32[3072,256]{0,1:T(8,128)S(1)}, f32[3072,256]{0,1:T(8,128)}, u32[]{:S(2)}) copy-start(f32[3072,256]{0,1:T(8,128)} %convolution_minimum_fusion) | copy-start | bytes 9437188
  456.6 10.3 %copy-start.12 = (bf16[1,32,32,512]{3,2,1,0:T(8,128)(2,1)S(1)}, bf16[1,32,32,512]{3,2,1,0:T(8,128)(2,1)}, u32[]{:S(2)}) copy-start(bf16[1,32,32,512]{3,2,1,0:T(8,128)(2,1)} %get-tuple-element.4) | copy-start | bytes 3145732
  456.6 10.3 %copy-start.17 = (bf16[3072,256]{0,1:T(8,128)(2,1)S(1)}, bf16[3072,256]{0,1:T(8,128)(2,1)}, u32[]{:S(2)}) copy-start(bf16[3072,256]{0,1:T(8,128)(2,1)} %fusion.11) | copy-start | bytes 4718596
  467.0 5.5 copy-start.11
  467.0 5.5 copy-start.18
  467.0 5.5 copy-start.19
  467.0 5.5 copy-start.20
  472.5 4.4 copy-start.10
  476.9 4.4 copy-start.9
  510.7 127.1 %copy-start.3 = (bf16[32,64,512]{2,1,0:T(8,128)(2,1)S(1)}, bf16[32,64,512]{2,1,0:T(8,128)(2,1)}, u32[]{:S(2)}) copy-start(bf16[32,64,512]{2,1,0:T(8,128)(2,1)} %slice.64) | copy-start | bytes 6291460
  633.6 11.7 %all-to-all-start.2 = ((bf16[96,4,512]{2,0,1:T(8,128)(2,1)}), bf16[96,4,512]{2,0,1:T(8,128)(2,1)S(1)}, u32[]{:S(2)}, u32[]{:S(2)}) async-start(bf16[96,4,512]{2,0,1:T(8,128)(2,1)} %copy.25), calls=%async_computation.2 | async-start | bytes 786432 | tf_op jit(solution)/shard_map/all_to_all | solution.py:56
  637.8 8.1 %copy-start.1 = (f32[384,4]{0,1:T(4,128)S(1)}, f32[384,4]{0,1:T(4,128)}, u32[]{:S(2)}) copy-start(f32[384,4]{0,1:T(4,128)} %param.9) | copy-start | bytes 18436
  (2 other events, 3.9 us)
Sparse Core Ops, SparseCore 0:
  115.4 44.0 all-gather.5
  161.4 126.1 all-gather.7
  290.0 86.2 all-gather.9
  507.4 123.8 reduce-scatter.3
where the time goes:
time: 657 us; the launch traced here: 653 us
  waiting for transfers between devices  345 us (53%)
  blocking collectives  128 us (19%)
  matrix products  109 us (17%)
  local copies, waits for them, and re-layouts  39.4 us (6%)
  between operations  14.2 us (2%)
  other arithmetic  12.4 us (2%)
    unnamed x5, waiting for transfers between devices  121 us
    all_to_all x1, blocking collectives, shards(): mine = lax.all_to_all(mine, FS, split_axis=0, concat_axis=0, tiled=True)  103 us
    all_gather x1, waiting for transfers between devices, shards(): wf = lax.all_gather(wk, 'tp', axis=0)  99.6 us
    all_gather x1, waiting for transfers between devices, shards(): xt = lax.all_gather(x, FS, axis=0)  78.2 us
    dot_general x4, matrix products, shards(): jnp.dot(flat, wf[t, :, :gate_rows, ff:].reshape(d, ff), preferred_element...  50.9 us
    all_gather x1, waiting for transfers between devices, shards(): wk = lax.all_gather(mine, 'gl', axis=1, tiled=True)  44.2 us
    dot_general x4, matrix products, shards(): jnp.dot(flat, wf[t, :, :gate_rows, :ff].reshape(d, ff), preferred_element...  39.8 us
    all_to_all x1, blocking collectives, shards(): call = lax.all_to_all(c, FS, split_axis=0, concat_axis=0, tiled=True)  24.9 us
  transfers between devices with their start and end apart: 5, of which 5 were waited for; matrix products, arithmetic and copies ran while one was open for 3% of the time, Pallas kernels for 0%

commit v1 on v0

v1 whole, which is shorter than its diff:
```python
import functools

import jax
import jax.numpy as jnp
from jax import lax
from jax.experimental import pallas as pl
from jax.experimental.pallas import tpu as pltpu
from jax.sharding import Mesh
from jax.sharding import PartitionSpec as P

LIMIT = 7.0
ALPHA = 1.702
EPS = 1e-06
FS = ("z", "core")
ROWS = ("gh", "gl", "z", "core")
MESH = pl.DeviceIdType.MESH
f32, bf16 = jnp.float32, jnp.bfloat16


def remote(src, dst, send, recv, where):
    return pltpu.make_async_remote_copy(
        src_ref=src, dst_ref=dst, send_sem=send, recv_sem=recv, device_id=where, device_id_type=MESH
    )


def apply_and_return(
    n_z, n_tp, wf, xt, ct, out, hid, cb, sib, acc_p, acc_s, fin,
    p_send, p_recv, s_send, s_recv, b_send, b_recv, f_send, f_recv,
):
    z, core, k = lax.axis_index("z"), lax.axis_index("core"), lax.axis_index("tp")
    steps = n_z // 2
    tok, width = xt.shape[1], xt.shape[2]
    sub = tok // 2
    cols = width // n_tp
    ffq = cols // 2
    gate_rows = width // wf.shape[1]
    down_rows = wf.shape[2] - gate_rows
    sign = 1 - 2 * core
    ahead = lax.rem(z + sign + n_z, n_z)
    behind = lax.rem(z - sign + n_z, n_z)
    sibling = {"core": 1 - core}

    def chips(i):
        j = steps - i
        first = lax.rem(z + j, n_z)
        second = jnp.where(i == 0, z, lax.rem(z - j + n_z, n_z))
        return first, second

    def inner(i):
        a, b = chips(i)
        x = jnp.concatenate(
            (
                xt[pl.ds(2 * a, 2)].reshape(2 * tok, width),
                xt[pl.ds(2 * b, 2)].reshape(2 * tok, width),
            ),
            axis=0,
        )
        for t in range(n_tp):
            gu = jnp.dot(x, wf[t, :, :gate_rows, :].reshape(width, cols), preferred_element_type=f32)
            g = jnp.minimum(gu[:, :ffq], LIMIT)
            u = jnp.clip(gu[:, ffq:], -LIMIT, LIMIT)
            hid[:, t * ffq : (t + 1) * ffq] = ((u + 1.0) * g * jax.nn.sigmoid(ALPHA * g)).astype(bf16)

    def outer(i):
        eye = lax.broadcasted_iota(jnp.int32, (tok, ct.shape[2]), 0) == lax.broadcasted_iota(
            jnp.int32, (tok, ct.shape[2]), 1
        )
        scales = []
        for chip in chips(i):
            for c in range(2):
                row = ct[2 * chip + c, pl.ds(2 * z + core, 1), :]
                scales.append(jnp.sum(jnp.where(eye, row, 0.0), axis=1, keepdims=True))
        scale = jnp.concatenate(scales, axis=0)
        for t in range(n_tp):
            down = wf[t, :, gate_rows:, :].reshape(wf.shape[1] * down_rows, cols)
            part = (scale * jnp.dot(hid[...], down, preferred_element_type=f32)).astype(bf16)
            for w in range(2):
                for c in range(2):
                    at = (2 * w + c) * tok
                    cb[i, w, c, :, t * cols : (t + 1) * cols] = part[at : at + tok]

    def to_sibling(i, w):
        return remote(cb.at[i, w, 1 - core], sib.at[i, w], b_send.at[i, w], b_recv.at[i, w], sibling)

    def hop_p(h, q):
        rows = pl.ds(q * sub, sub)
        return remote(
            acc_p.at[h, rows], acc_p.at[h + 1, rows], p_send.at[h, q], p_recv.at[h + 1, q], {"z": ahead}
        )

    def hop_s(h, q):
        rows = pl.ds(q * sub, sub)
        return remote(
            acc_s.at[h, rows], acc_s.at[h + 1, rows], s_send.at[h, q], s_recv.at[h + 1, q], {"z": behind}
        )

    def local(h, w, rows):
        return cb[h, w, core, rows, :].astype(f32) + sib[h, w, rows, :].astype(f32)

    def combine(h, q):
        rows = pl.ds(q * sub, sub)
        prim = jnp.where(h == 0, 0, core)

        @pl.when(h == 0)
        def _():
            acc_p[h, rows, :] = local(h, prim, rows).astype(bf16)

        @pl.when(h > 0)
        def _():
            hop_p(h - 1, q).wait_recv()
            acc_p[h, rows, :] = (local(h, prim, rows) + acc_p[h, rows, :].astype(f32)).astype(bf16)

        hop_p(h, q).start()

        @pl.when(h == 1)
        def _():
            acc_s[h, rows, :] = local(h, 1 - core, rows).astype(bf16)

        @pl.when(h > 1)
        def _():
            hop_s(h - 1, q).wait_recv()
            acc_s[h, rows, :] = (local(h, 1 - core, rows) + acc_s[h, rows, :].astype(f32)).astype(bf16)

        @pl.when(h > 0)
        def _():
            hop_s(h, q).start()

    def sib_in(i):
        for w in range(2):
            to_sibling(i, w).wait_recv()

    def body(i, carry):
        @pl.when(i > 0)
        def _():
            sib_in(i - 1)
            combine(i - 1, 0)

        inner(i)

        @pl.when(i > 0)
        def _():
            combine(i - 1, 1)

        outer(i)
        for w in range(2):
            to_sibling(i, w).start()
        return carry

    lax.fori_loop(0, steps, body, 0)
    sib_in(steps - 1)
    combine(steps - 1, 0)
    combine(steps - 1, 1)

    def to_tp(t):
        return remote(
            fin.at[t], out.at[pl.ds(pl.multiple_of(k * tok, tok), tok)], f_send.at[t], f_recv.at[k], {"tp": t}
        )

    for q in range(2):
        rows = pl.ds(q * sub, sub)
        hop_p(steps - 1, q).wait_recv()
        hop_s(steps - 1, q).wait_recv()
        total = (
            local(0, 1, rows)
            + acc_p[steps, rows, :].astype(f32)
            + acc_s[steps, rows, :].astype(f32)
        ).astype(bf16)
        for t in range(n_tp):
            fin[t, rows, :] = total[:, t * cols : (t + 1) * cols]
    for step in range(1, n_tp):
        to_tp(lax.rem(k + step, n_tp)).start()
    out[pl.ds(pl.multiple_of(k * tok, tok), tok), :] = fin[k]

    def drain(h, carry):
        for q in range(2):
            hop_p(h, q).wait_send()

            @pl.when(h > 0)
            def _():
                hop_s(h, q).wait_send()

        for w in range(2):
            to_sibling(h, w).wait_send()
        return carry

    lax.fori_loop(0, steps, drain, 0)
    for step in range(1, n_tp):
        t = lax.rem(k + step, n_tp)
        to_tp(t).wait_send()
        back = lax.rem(k + n_tp - step, n_tp)
        remote(
            fin.at[k], out.at[pl.ds(pl.multiple_of(back * tok, tok), tok)], f_send.at[t], f_recv.at[back], {"tp": t}
        ).wait_recv()


def apply_scratch(n_z, n_tp, n_fs, tok, width):
    steps = n_z // 2
    dma = pltpu.SemaphoreType.DMA
    return [
        pltpu.VMEM((4 * tok, width // 2), bf16),
        pltpu.VMEM((steps, 2, 2, tok, width), bf16),
        pltpu.VMEM((steps, 2, tok, width), bf16),
        pltpu.VMEM((steps + 1, tok, width), bf16),
        pltpu.VMEM((steps + 1, tok, width), bf16),
        pltpu.VMEM((n_tp, tok, width // n_tp), bf16),
        dma((steps, 2)), dma((steps + 1, 2)), dma((steps, 2)), dma((steps + 1, 2)),
        dma((steps, 2)), dma((steps, 2)), dma((n_tp,)), dma((n_tp,)),
    ]


def bring(
    n_z, n_tp, n_gl, w, xq, cq, wf, xt, ct, tbp, tbs,
    zp_send, zp_recv, zs_send, zs_recv, fz_send, wz_recv, y_send, y_recv, x_send, x_recv, r_send, r_recv,
    tp_send, tp_recv, ts_send, ts_recv, tb_send, tb_recv, l_sem, ws_send, ws_recv,
):
    z, core, k, p = (lax.axis_index(a) for a in ("z", "core", "tp", "gl"))
    top = n_z // 2
    me = 2 * z + core
    sign = 1 - 2 * core
    half = w.shape[1] // n_gl
    sub = xq.shape[0] // 2
    steps = {True: sign, False: -sign}
    length = {True: top, False: top - 1}
    transit = {True: tbp, False: tbs}
    z_send = {True: zp_send, False: zs_send}
    z_recv = {True: zp_recv, False: zs_recv}
    sibling = {"core": 1 - core}

    def chip(v):
        return lax.rem(z + v + 2 * n_z, n_z)

    def rows(q):
        return pl.ds(pl.multiple_of(q * half, half), half)

    def pair(zs):
        return pl.ds(2 * zs, 2)

    def tri(prim, h, j):
        return h * length[prim] - h * (h - 1) // 2 + j - 1

    def landed(prim, h, j):
        return transit[prim].at[tri(prim, h, j) - length[prim]]

    def z_move(prim, h, j):
        step = steps[prim]
        src = w.at[pair(chip(step * j)), rows(p)] if h == 0 else landed(prim, h, j)
        return remote(
            src, landed(prim, h + 1, j - 1), z_send[prim].at[tri(prim, h, j)],
            z_recv[prim].at[tri(prim, h + 1, j - 1)], {"z": chip(step)},
        )

    def z_wait(prim, h, j):
        here = landed(prim, h, j)
        at = tri(prim, h, j)
        remote(here, here, z_send[prim].at[at], z_recv[prim].at[at], {"z": chip(steps[prim])}).wait_recv()

    def z_final(prim, h, c2):
        step = steps[prim]
        src = w.at[2 * chip(step) + c2, rows(p)] if h == 0 else landed(prim, h, 1).at[c2]
        slot = 2 * chip(-step * h) + core
        return remote(
            src, wf.at[k, slot, rows(p)], fz_send.at[0 if prim else 1, h, c2], wz_recv.at[slot],
            {"z": chip(step), "core": c2},
        )

    def to_pair(zs, q):
        return remote(
            wf.at[k, pair(zs), rows(q)], wf.at[k, pair(zs), rows(q)], y_send.at[zs], y_recv.at[zs], {"gl": 1 - p}
        )

    def x_move(d, slot, zs, q):
        return remote(
            wf.at[slot, pair(zs), rows(q)], wf.at[slot, pair(zs), rows(q)], x_send.at[d, zs, q],
            x_recv.at[d, zs, q], {"tp": lax.rem(k + (1, n_tp - 1)[d], n_tp)},
        )

    def x_from(d):
        return lax.rem(k + (n_tp - 1, 1)[d], n_tp)

    def x_both(zs, q):
        x_move(0, k, zs, q).start()
        x_move(1, k, zs, q).start()

    def x_pass(d, slot, zs, q):
        return remote(
            wf.at[slot, pair(zs), rows(q)], wf.at[slot, pair(zs), rows(q)], r_send.at[zs, q], r_recv.at[zs, q],
            {"tp": lax.rem(k + (1, n_tp - 1)[d], n_tp)},
        )

    def relay(zs, q):
        if n_gl == 1:
            x_move(0, x_from(0), zs, q).wait_recv()
            x_pass(0, x_from(0), zs, q).start()
            return
        for d in range(2):

            @pl.when(q == d)
            def _():
                x_move(d, x_from(d), zs, d).wait_recv()
                x_pass(d, x_from(d), zs, d).start()

    def chips_at(level):
        if level == 0:
            return [z]
        if level == top:
            return [chip(top)]
        return [chip(-level), chip(level)]

    def arrive(level):
        for zs in chips_at(level):
            for c2 in range(2):
                slot = 2 * zs + c2
                here = wf.at[k, slot, rows(p)]
                remote(here, here, fz_send.at[0, 0, c2], wz_recv.at[slot], sibling).wait_recv()
            if n_gl == 2:
                to_pair(zs, p).start()
            x_both(zs, p)

    def other_half(level):
        if n_gl == 2:
            for zs in chips_at(level):
                to_pair(zs, 1 - p).wait_recv()
                x_both(zs, 1 - p)

    def forward(level, first, last):
        def one(j, carry):
            for prim in (True, False):

                @pl.when(j <= length[prim] - level)
                def _():
                    if level > 0:
                        z_wait(prim, level, j)
                    z_move(prim, level, j).start()

            return carry

        if first < last:
            lax.fori_loop(first, last, one, 0)

    def deliver(level):
        for prim in (True, False):
            if level < length[prim]:
                if level > 0:
                    z_wait(prim, level, 1)
                for c2 in range(2):
                    z_final(prim, level, c2).start()

    def part(ref, slot, q):
        return ref.at[slot, pl.ds(q * sub, sub)]

    def token(slot, q):
        return ct.at[slot] if q == 2 else part(xt, slot, q)

    def mine(q):
        return cq if q == 2 else xq.at[pl.ds(q * sub, sub)]

    t_send = {True: tp_send, False: ts_send}
    t_recv = {True: tp_recv, False: ts_recv}

    def t_move(prim, h, q):
        step = steps[prim]
        slot = 2 * chip(-step * h) + core
        return remote(
            mine(q) if h == 0 else token(slot, q), token(slot, q), t_send[prim].at[h, q],
            t_recv[prim].at[h + 1, q], {"z": chip(step)},
        )

    def t_wait(prim, h, q):
        here = token(2 * chip(-steps[prim] * h) + core, q)
        remote(here, here, t_send[prim].at[0, q], t_recv[prim].at[h, q], sibling).wait_recv()

    def t_sibling(zs, q, own=False):
        slot = 2 * zs + core
        return remote(mine(q) if own else token(slot, q), token(slot, q), tb_send.at[zs, q], tb_recv.at[zs, q], sibling)

    def t_own(q):
        return pltpu.make_async_copy(mine(q), token(me, q), l_sem.at[1 + q])

    def tokens_out():
        for q in (2, 0, 1):
            for prim in (True, False):
                if length[prim] > 0:
                    t_move(prim, 0, q).start()
        for q in (2, 0, 1):
            t_sibling(z, q, True).start()
            t_own(q).start()

    def tokens_at(h):
        for q in (2, 0, 1):
            for prim in (True, False):
                if h <= length[prim]:
                    t_wait(prim, h, q)
                    if h < length[prim]:
                        t_move(prim, h, q).start()
                    t_sibling(chip(-steps[prim] * h), q).start()

    def own_block():
        return pltpu.make_async_copy(w.at[me], wf.at[k, me], l_sem.at[0])

    def sib_block(sender):
        return remote(w.at[2 * z + 1 - core], wf.at[k, sender], ws_send, ws_recv, sibling)

    settled = max(top - 4, 0)
    late = []
    for level in range(settled + 1, top + 1):
        late += [(level, 0)] + ([(level, 1)] if n_gl == 2 else [])

    def one_late():
        if late:
            level, turn = late.pop(0)
            for zs in chips_at(level):
                relay(zs, lax.rem(p + turn, n_gl))

    own_block().start()
    sib_block(me).start()
    deliver(0)
    forward(0, 2, top + 1)
    own_block().wait()
    sib_block(me + 1 - 2 * core).wait_recv()
    for q in range(n_gl):
        x_both(z, q)
    if top - 2 < 1:
        tokens_out()
    for level in range(1, top + 1):
        arrive(level)
        deliver(level)
        if level == 1:
            for q in range(n_gl):
                relay(z, q)
        elif level - 1 <= settled and n_gl == 2:
            for zs in chips_at(level - 1):
                relay(zs, 1 - p)
        forward(level, 2, min(4, top - level + 1))
        if level < top:
            other_half(level)
        if level <= settled:
            for zs in chips_at(level):
                relay(zs, p)
        forward(level, 4, top - level + 1)
        if level == top - 2:
            tokens_out()
            one_late()
        if level == top:
            one_late()
    for h in range(1, top + 1):
        tokens_at(h)
        if h == 1:
            other_half(top)
            if settled + 1 == top:
                pass
        one_late()
    while late:
        one_late()

    def settle(zs, carry):
        @pl.when(zs != z)
        def _():
            pass

        if n_gl == 2:
            x_move(0, x_from(0), zs, 1).wait_recv()
        x_move(1, x_from(1), zs, 0).wait_recv()
        for q in range(n_gl):
            x_pass(q, lax.rem(k + 2, n_tp), zs, q).wait_recv()
        for q in range(3):
            here = token(2 * zs + 1 - core, q)
            remote(here, here, tb_send.at[zs, q], tb_recv.at[zs, q], sibling).wait_recv()
        return carry

    lax.fori_loop(0, n_z, settle, 0)
    for q in range(3):
        t_own(q).wait()

    def drain():
        sib_block(me).wait_send()

        def by_chip(zs, carry):
            for q in range(n_gl):
                x_move(0, k, zs, q).wait_send()
                x_move(1, k, zs, q).wait_send()
                x_pass(0, k, zs, q).wait_send()
            if n_gl == 2:

                @pl.when(zs != z)
                def _():
                    to_pair(zs, p).wait_send()

            for q in range(3):
                t_sibling(zs, q).wait_send()
            return carry

        lax.fori_loop(0, n_z, by_chip, 0)
        for prim in (True, False):
            for h in range(length[prim]):
                for c2 in range(2):
                    z_final(prim, h, c2).wait_send()
                for q in range(3):
                    t_move(prim, h, q).wait_send()

                def moved(j, carry):
                    z_move(prim, h, j).wait_send()
                    return carry

                if length[prim] - h >= 2:
                    lax.fori_loop(2, length[prim] - h + 1, moved, 0)

    return drain


def bring_scratch(n_z, n_tp, n_gl, w, xq, cq):
    top, n_fs = n_z // 2, 2 * n_z
    dma = pltpu.SemaphoreType.DMA
    prim, sec = top * (top + 1) // 2, top * (top - 1) // 2
    half = w[1] // n_gl
    return [
        pltpu.VMEM((n_tp, n_fs) + w[1:], bf16),
        pltpu.VMEM((n_fs,) + xq, bf16),
        pltpu.VMEM((n_fs,) + cq, f32),
        pltpu.VMEM((prim - top, 2, half, w[2]), bf16),
        pltpu.VMEM((max(sec - top + 1, 1), 2, half, w[2]), bf16),
        dma((prim,)), dma((prim,)), dma((max(sec, 1),)), dma((max(sec, 1),)),
        dma((2, top, 2)), dma((n_fs,)), dma((n_z,)), dma((n_z,)),
        dma((2, n_z, n_gl)), dma((2, n_z, n_gl)), dma((n_z, n_gl)), dma((n_z, n_gl)),
        dma((top, 3)), dma((top + 1, 3)), dma((top, 3)), dma((top + 1, 3)),
        dma((n_z, 3)), dma((n_z, 3)), dma((4,)), dma(()), dma(()),
    ]


def whole_kernel(n_z, n_tp, n_gl, n_bring, w, xq, cq, gate_out, up_out, down_out, mixed_out, *scratch):
    z, core, k, p = (lax.axis_index(a) for a in ("z", "core", "tp", "gl"))
    barrier = pltpu.get_barrier_semaphore()
    peers = [{"z": lax.rem(z + d, n_z), "core": c} for d in (1, n_z - 1) for c in range(2)]
    peers += [{"core": 1 - core}] + [{"tp": lax.rem(k + step, n_tp)} for step in range(1, n_tp)]
    if n_gl == 2:
        peers += [{"gl": 1 - p}]
    for peer in peers:
        pl.semaphore_signal(barrier, inc=1, device_id=peer, device_id_type=MESH)
    pl.semaphore_wait(barrier, len(peers))
    for_bring, for_apply, out_sem = scratch[:n_bring], scratch[n_bring:-1], scratch[-1]
    wf, xt, ct = for_bring[:3]
    drain = bring(n_z, n_tp, n_gl, w, xq, cq, *for_bring)
    gate_rows, ffq = gate_out.shape[1:]
    share, cols = down_out.shape[0], wf.shape[3]
    outs = [
        pltpu.make_async_copy(wf.at[k, :, :gate_rows, :ffq], gate_out, out_sem.at[0]),
        pltpu.make_async_copy(wf.at[k, :, :gate_rows, ffq:], up_out, out_sem.at[1]),
    ]
    for t in range(n_tp):
        outs.append(
            pltpu.make_async_copy(
                wf.at[t, pl.ds(k * share, share), gate_rows:, :],
                down_out.at[:, :, t * cols : (t + 1) * cols],
                out_sem.at[2 + t],
            )
        )
    for copy in outs:
        copy.start()
    apply_and_return(n_z, n_tp, wf, xt, ct, mixed_out, *for_apply)
    for copy in outs:
        copy.wait()
    drain()


def shards(prompt, routes, route_weight, norm_gain, gate_train, up_train, down_train):
    n_tp, n_z, n_gl = lax.axis_size("tp"), lax.axis_size("z"), lax.axis_size("gl")
    n_fs = 2 * n_z
    k = lax.axis_index("tp")
    experts, gate_rows, ffq = gate_train.shape
    down_rows, cols = down_train.shape[1:]
    gate = (norm_gain[None, :, None] * gate_train).astype(bf16)
    up = (norm_gain[None, :, None] * up_train).astype(bf16)
    both = jnp.concatenate((gate, up), axis=2)
    w = jnp.concatenate((both, down_train.astype(bf16)), axis=1)
    tok = prompt.shape[0] // n_tp
    x = lax.dynamic_slice_in_dim(prompt, k * tok, tok, 0).astype(f32)
    x = (x * lax.rsqrt(jnp.mean(x * x, axis=-1, keepdims=True) + EPS)).astype(bf16)
    r = lax.dynamic_slice_in_dim(routes, k * tok, tok, 0)
    rw = lax.dynamic_slice_in_dim(route_weight, k * tok, tok, 0)
    hot = r[:, :, None] == jnp.arange(experts, dtype=jnp.int32)[None, None, :]
    c = jnp.sum(jnp.where(hot, rw[:, :, None], 0.0), axis=1).T
    c = jnp.pad(c, ((0, 0), (0, -tok % 128)))
    d = x.shape[1]
    share = n_fs // n_tp
    vmem = pl.BlockSpec(memory_space=pltpu.VMEM)
    hbm = pl.BlockSpec(memory_space=pl.ANY)
    for_bring = bring_scratch(n_z, n_tp, n_gl, w.shape, x.shape, c.shape)
    gate_own, up_own, down_own, mixed = pl.pallas_call(
        functools.partial(whole_kernel, n_z, n_tp, n_gl, len(for_bring)),
        out_shape=(
            jax.ShapeDtypeStruct((n_fs, gate_rows, ffq), bf16),
            jax.ShapeDtypeStruct((n_fs, gate_rows, ffq), bf16),
            jax.ShapeDtypeStruct((share, down_rows, n_tp * cols), bf16),
            jax.ShapeDtypeStruct((tok * n_tp, cols), bf16),
        ),
        in_specs=[vmem] * 3,
        out_specs=(hbm, hbm, hbm, vmem),
        scratch_shapes=for_bring
        + apply_scratch(n_z, n_tp, n_fs, tok, d)
        + [pltpu.SemaphoreType.DMA((2 + n_tp,))],
        compiler_params=pltpu.CompilerParams(
            collective_id=0, has_side_effects=True, vmem_limit_bytes=67043328
        ),
    )(w, x, c)
    return (
        gate_own.reshape(1, d, ffq),
        up_own.reshape(1, d, ffq),
        down_own.reshape(1, share * down_rows, n_tp * cols),
        mixed,
    )


def solution(mesh):
    groups, n_tp = mesh.shape["grp"], mesh.shape["tp"]
    chips = mesh.shape["fs"] // 2
    pair = 2 if groups % 2 == 0 else 1
    finer = Mesh(
        mesh.devices.reshape(groups // pair, pair, chips, 2, n_tp),
        ("gh", "gl", "z", "core", "tp"),
    )
    return jax.shard_map(
        shards,
        mesh=finer,
        in_specs=(P(ROWS), P(ROWS), P(ROWS), P(FS), P(None, FS, "tp"), P(None, FS, "tp"), P(None, FS, "tp")),
        out_specs=(P(ROWS, None, "tp"), P(ROWS, None, "tp"), P(ROWS, "tp", None), P(ROWS, "tp")),
        check_vma=False,
    )
```

time: 657 us -> 278 us (0.42)
  waiting for transfers between devices: 345 us -> 0 us
  Pallas kernels: 0 us -> 261 us
  blocking collectives: 128 us -> 0 us
  matrix products: 109 us -> 0 us
  local copies, waits for them, and re-layouts: 39.4 us -> 7.4 us
  between operations: 14.2 us -> 0.74 us
    pallas_call x0 -> x1, Pallas kernels: none -> 261 us  [shards(): pl.pallas_call(functools.partial(whole_kernel, n_z, n_tp, n_gl, len(for_b...]
    all_gather x3 -> x0, waiting for transfers between devices: 222 us -> none  [the longest x1 99.6 us: shards(): wf = lax.all_gather(wk, 'tp', axis=0)]
    all_to_all x2 -> x0, blocking collectives: 128 us -> none  [the longest x1 103 us: shards(): mine = lax.all_to_all(mine, FS, split_axis=0, concat_axis=0, tiled=True)]
    unnamed x5 -> x0, waiting for transfers between devices: 121 us -> none
    dot_general x12 -> x0, matrix products: 109 us -> none  [the longest x4 50.9 us: shards(): jnp.dot(flat, wf[t, :, :gate_rows, ff:].reshape(d, ff), preferred_element...]
    slice x5 -> x0, local copies, waits for them, and re-layouts: 14.8 us -> none  [the longest x1 6.06 us: shards(): wf[t, :, :gate_rows, ff:].reshape(d, ff)]
    unnamed x45 -> x16, local copies, waits for them, and re-layouts: 19.9 us -> 5.12 us
  transfers between devices with their start and end apart: 5 -> 0, of which waited for: 5 -> 0; matrix products, arithmetic and copies ran while one was open for 3% -> 0% of each run, Pallas kernels for 0% -> 0%
where the time goes in v1:
time: 278 us; the launch traced here: 277 us
  Pallas kernels  261 us (94%)
  other arithmetic  7.41 us (3%)
  local copies, waits for them, and re-layouts  7.4 us (3%)
    pallas_call x1, Pallas kernels, shards(): pl.pallas_call(functools.partial(whole_kernel, n_z, n_tp, n_gl, len(for_b...  261 us

profile of v1, /device:TPU:40, one launch (start us, length us, event | category | flops | bytes accessed | tf_op | source)
XLA Modules:
  0.0 276.7 jit_solution(3513580608431044562)
XLA Ops:
  0.6 0.0 copy-start.1
  0.6 1.3 fusion
  2.0 0.0 copy-start
  2.0 0.0 copy-start.5
  2.0 0.9 constant_dynamic-slice_fusion.1
  2.9 0.8 constant_dynamic-slice_fusion
  3.7 0.6 pad.4.cq
  4.3 1.9 fusion.1.xq
  6.2 1.7 convert_element_type.19
  7.9 0.0 copy-done.1
  7.9 0.0 copy-done
  8.0 0.0 copy-done.5
  8.0 0.6 multiply_convert_fusion.1
  8.6 1.8 pad_maximum_fusion.w
  10.4 261.2 %shard_map.102 = (bf16[32,64,256]{2,1,0:T(8,128)(2,1)}, bf16[32,64,256]{2,1,0:T(8,128)(2,1)}, bf16[8,32,2048]{2,1,0:T(8,128)(2,1)}, bf16[384,512]{1,0:T(8,128)(2,1)}) custom-call(bf16[32,96,512]{2,1,0:T(8,128)(2,1)} %pad_maximum_fusion.w, bf16[96,2048]{1,0:T(8,128)(2,1)} %fusion.1.xq, f32[32,128]{1,0:T(8,128)} %pad.4.cq), custom_call_target="tpu_custom_call" | custom-call | tf_op jit(solution)/shard_map/pallas_call | solution.py:587
  271.6 0.0 copy-start.3
  271.6 0.0 copy-start.2
  271.6 2.4 copy.17
  274.0 0.0 copy-done.3
  274.0 1.0 copy.18
  275.0 0.0 copy-done.2
  275.0 1.0 copy.19
  276.0 0.0 copy-done.4
  276.0 0.7 copy.20
  (3 shorter events, 0.0 us)
Async XLA Ops:
  0.6 7.3 %copy-start.1 = (f32[32,64,256]{2,1,0:T(8,128)S(1)}, f32[32,64,256]{2,1,0:T(8,128)}, u32[]{:S(2)}) copy-start(f32[32,64,256]{2,1,0:T(8,128)} %param.12) | copy-start | bytes 6291460
  2.0 6.0 %copy-start = (f32[32,64,256]{2,1,0:T(8,128)S(1)}, f32[32,64,256]{2,1,0:T(8,128)}, u32[]{:S(2)}) copy-start(f32[32,64,256]{2,1,0:T(8,128)} %param.11) | copy-start | bytes 6291460
  2.0 6.0 %copy-start.5 = (f32[64]{0:T(128)S(1)}, f32[64]{0:T(128)}, u32[]{:S(2)}) copy-start(f32[64]{0:T(128)} %param.10) | copy-start | bytes 772
  271.6 2.4 copy-start.3
  271.6 3.4 %copy-start.2 = (bf16[8,32,2048]{2,1,0:T(8,128)(2,1)S(1)}, bf16[8,32,2048]{2,1,0:T(8,128)(2,1)}, u32[]{:S(2)}) copy-start(bf16[8,32,2048]{2,1,0:T(8,128)(2,1)} %get-tuple-element.10) | copy-start | bytes 3145732
  274.0 1.9 copy-start.4

commit v2 on v1

v2 whole, which is shorter than its diff:
```python
import functools

import jax
import jax.numpy as jnp
from jax import lax
from jax.experimental import pallas as pl
from jax.experimental.pallas import tpu as pltpu
from jax.sharding import Mesh
from jax.sharding import PartitionSpec as P

LIMIT = 7.0
ALPHA = 1.702
EPS = 1e-06
FS = ("z", "core")
ROWS = ("gh", "gl", "z", "core")
MESH = pl.DeviceIdType.MESH
f32, bf16 = jnp.float32, jnp.bfloat16


def remote(src, dst, send, recv, where):
    return pltpu.make_async_remote_copy(
        src_ref=src, dst_ref=dst, send_sem=send, recv_sem=recv, device_id=where, device_id_type=MESH
    )


def apply_and_return(
    n_z, n_tp, wf, xt, ct, out, hid, cb, sib, acc_p, acc_s, fin,
    p_send, p_recv, s_send, s_recv, b_send, b_recv, f_send, f_recv,
):
    z, core, k = lax.axis_index("z"), lax.axis_index("core"), lax.axis_index("tp")
    steps = n_z // 2
    tok, width = xt.shape[1], xt.shape[2]
    sub = tok // 2
    cols = width // n_tp
    ffq = cols // 2
    gate_rows = width // wf.shape[1]
    down_rows = wf.shape[2] - gate_rows
    sign = 1 - 2 * core
    ahead = lax.rem(z + sign + n_z, n_z)
    behind = lax.rem(z - sign + n_z, n_z)
    sibling = {"core": 1 - core}

    def chips(i):
        j = steps - i
        return lax.rem(z + j, n_z), lax.rem(z - j + n_z, n_z)

    def inner(some):
        x = jnp.concatenate([xt[pl.ds(2 * chip, 2)].reshape(2 * tok, width) for chip in some], axis=0)
        count = x.shape[0]
        for t in range(n_tp):
            gu = jnp.dot(x, wf[t, :, :gate_rows, :].reshape(width, cols), preferred_element_type=f32)
            g = jnp.minimum(gu[:, :ffq], LIMIT)
            u = jnp.clip(gu[:, ffq:], -LIMIT, LIMIT)
            hid[:count, t * ffq : (t + 1) * ffq] = ((u + 1.0) * g * jax.nn.sigmoid(ALPHA * g)).astype(bf16)

    def outer(some, places):
        count = 2 * tok * len(some)
        eye = lax.broadcasted_iota(jnp.int32, (tok, ct.shape[2]), 0) == lax.broadcasted_iota(
            jnp.int32, (tok, ct.shape[2]), 1
        )
        scales = []
        for chip in some:
            for c in range(2):
                row = ct[2 * chip + c, pl.ds(2 * z + core, 1), :]
                scales.append(jnp.sum(jnp.where(eye, row, 0.0), axis=1, keepdims=True))
        scale = jnp.concatenate(scales, axis=0)
        for t in range(n_tp):
            down = wf[t, :, gate_rows:, :].reshape(wf.shape[1] * down_rows, cols)
            part = (scale * jnp.dot(hid[:count, :], down, preferred_element_type=f32)).astype(bf16)
            for n, (i, w) in enumerate(places):
                for c in range(2):
                    at = (2 * n + c) * tok
                    cb[i, w, c, :, t * cols : (t + 1) * cols] = part[at : at + tok]

    def b_slot(i, w):
        return steps * w if isinstance(i, int) and i == 0 else i

    def to_sibling(i, w):
        return remote(cb.at[i, w, 1 - core], sib.at[i, w], b_send, b_recv.at[b_slot(i, w)], sibling)

    def hop_p(h, q):
        rows = pl.ds(q * sub, sub)
        return remote(
            acc_p.at[h, rows], acc_p.at[h + 1, rows], p_send, p_recv.at[h, q], {"z": ahead}
        )

    def hop_s(h, q):
        rows = pl.ds(q * sub, sub)
        return remote(
            acc_s.at[h, rows], acc_s.at[h + 1, rows], s_send, s_recv.at[h - 1, q], {"z": behind}
        )

    def local(h, w, rows):
        return cb[h, w, core, rows, :].astype(f32) + sib[h, w, rows, :].astype(f32)

    def combine_p(h, q):
        rows = pl.ds(q * sub, sub)
        prim = jnp.where(h == 0, 0, core)

        @pl.when(h == 0)
        def _():
            acc_p[h, rows, :] = local(h, prim, rows).astype(bf16)

        @pl.when(h > 0)
        def _():
            hop_p(h - 1, q).wait_recv()
            acc_p[h, rows, :] = (local(h, prim, rows) + acc_p[h, rows, :].astype(f32)).astype(bf16)

        hop_p(h, q).start()

    def combine_s(h, q):
        rows = pl.ds(q * sub, sub)

        @pl.when(h == 1)
        def _():
            acc_s[h, rows, :] = local(h, 1 - core, rows).astype(bf16)

        @pl.when(h > 1)
        def _():
            hop_s(h - 1, q).wait_recv()
            acc_s[h, rows, :] = (local(h, 1 - core, rows) + acc_s[h, rows, :].astype(f32)).astype(bf16)

        hop_s(h, q).start()

    def sib_in(i):
        remote(sib.at[i], sib.at[i], b_send, b_recv.at[i], sibling).wait_recv()

    def sib_out(i):
        for w in range(2):
            to_sibling(i, w).start()

    def body(i, carry):
        sib_in(i)
        combine_s(i, 0)

        @pl.when(i == 1)
        def _():
            combine_s(i, 1)
            to_sibling(0, 0).wait_recv()

        combine_p(i - 1, 0)

        @pl.when(i == 1)
        def _():
            combine_p(i - 1, 1)

        inner(chips(i + 1))

        @pl.when(i > 1)
        def _():
            combine_s(i, 1)
            combine_p(i - 1, 1)

        outer(chips(i + 1), [(i + 1, 0), (i + 1, 1)])
        sib_out(i + 1)
        return carry

    def one_chip(chip, w):
        inner([chip])
        outer([chip], [(0, w)])
        to_sibling(0, w).start()

    def to_tp(t, q):
        rows = pl.ds(q * sub, sub)
        at = pl.multiple_of(k * tok + q * sub, sub)
        return remote(fin.at[t, rows], out.at[pl.ds(at, sub)], f_send, f_recv, {"tp": t})

    def sent(ref, sem):
        remote(ref, ref, sem, sem, sibling).wait_send()

    def first():
        one_chip(z, 1)

    def second():
        inner(chips(1))

    def third():
        outer(chips(1), [(1, 0), (1, 1)])
        sib_out(1)

    def rest(drain_bring):
        one_chip(lax.rem(z + steps, n_z), 0)
        lax.fori_loop(1, steps - 1, body, 0)
        last = steps - 1
        sib_in(last)
        if last == 1:
            to_sibling(0, 0).wait_recv()
        for q in range(2):
            combine_s(last, q)
            combine_p(last - 1, q)
        for q in range(2):
            combine_p(last, q)
        to_sibling(0, 1).wait_recv()
        drain_bring()
        sent(sib, b_send)
        for q in range(2):
            rows = pl.ds(q * sub, sub)
            hop_p(steps - 1, q).wait_recv()
            hop_s(steps - 1, q).wait_recv()
            total = (
                local(0, 1, rows)
                + acc_p[steps, rows, :].astype(f32)
                + acc_s[steps, rows, :].astype(f32)
            ).astype(bf16)
            for t in range(n_tp):
                fin[t, rows, :] = total[:, t * cols : (t + 1) * cols]
            for step in (2, 1, 3):
                to_tp(lax.rem(k + step, n_tp), q).start()
            out[pl.ds(pl.multiple_of(k * tok + q * sub, sub), sub), :] = fin[k, rows, :]
        sent(acc_p.at[pl.ds(0, steps)], p_send)
        sent(acc_s.at[pl.ds(0, steps - 1)], s_send)
        peers = fin.at[pl.ds(0, n_tp - 1)]
        sent(peers, f_send)
        remote(peers, peers, f_send, f_recv, sibling).wait_recv()

    return first, second, third, rest


def apply_scratch(n_z, n_tp, n_fs, tok, width):
    steps = n_z // 2
    dma = pltpu.SemaphoreType.DMA
    return [
        pltpu.VMEM((4 * tok, width // 2), bf16),
        pltpu.VMEM((steps, 2, 2, tok, width), bf16),
        pltpu.VMEM((steps, 2, tok, width), bf16),
        pltpu.VMEM((steps + 1, tok, width), bf16),
        pltpu.VMEM((steps + 1, tok, width), bf16),
        pltpu.VMEM((n_tp, tok, width // n_tp), bf16),
        dma(()), dma((steps, 2)), dma(()), dma((steps - 1, 2)), dma(()), dma((steps + 1,)), dma(()), dma(()),
    ]


def bring(
    n_z, n_tp, n_gl, prepare, first, second, third, w, xq, cq, wf, xt, ct, tbp, tbs,
    zp_send, zp_recv, zs_send, zs_recv, fz_send, wz_recv, y_send, y_recv, x_send, x_recv, r_send,
    t_send, tp_recv, ts_recv, tb_send, tb_recv, l_sem, ws_send, ws_recv,
):
    z, core, k, p = (lax.axis_index(a) for a in ("z", "core", "tp", "gl"))
    top = n_z // 2
    me = 2 * z + core
    sign = 1 - 2 * core
    half = w.shape[1] // n_gl
    sub = xq.shape[0] // 2
    steps = {True: sign, False: -sign}
    length = {True: top, False: top - 1}
    transit = {True: tbp, False: tbs}
    z_send = {True: zp_send, False: zs_send}
    z_recv = {True: zp_recv, False: zs_recv}
    sibling = {"core": 1 - core}

    def chip(v):
        return lax.rem(z + v + 2 * n_z, n_z)

    def rows(q):
        return pl.ds(pl.multiple_of(q * half, half), half)

    def pair(zs):
        return pl.ds(2 * zs, 2)

    def tri(prim, h, j):
        return h * length[prim] - h * (h - 1) // 2 + j - 1

    def landed(prim, h, j):
        return transit[prim].at[tri(prim, h, j) - length[prim]]

    def z_move(prim, h, j):
        step = steps[prim]
        src = w.at[pair(chip(step * j)), rows(p)] if h == 0 else landed(prim, h, j)
        return remote(
            src, landed(prim, h + 1, j - 1), z_send[prim],
            z_recv[prim].at[tri(prim, h + 1, j - 1) - length[prim]], {"z": chip(step)},
        )

    def z_wait(prim, h, j):
        here = landed(prim, h, j)
        at = tri(prim, h, j) - length[prim]
        remote(here, here, z_send[prim], z_recv[prim].at[at], {"z": chip(steps[prim])}).wait_recv()

    def z_final(prim, h, c2):
        step = steps[prim]
        src = w.at[2 * chip(step) + c2, rows(p)] if h == 0 else landed(prim, h, 1).at[c2]
        slot = 2 * chip(-step * h) + core
        return remote(
            src, wf.at[k, slot, rows(p)], fz_send, wz_recv.at[chip(-step * h)],
            {"z": chip(step), "core": c2},
        )

    def to_pair(zs, q):
        return remote(
            wf.at[k, pair(zs), rows(q)], wf.at[k, pair(zs), rows(q)], y_send, y_recv.at[zs], {"gl": 1 - p}
        )

    def x_move(d, slot, zs, q):
        return remote(
            wf.at[slot, pair(zs), rows(q)], wf.at[slot, pair(zs), rows(q)], x_send,
            x_recv.at[(1 - (q + d) % 2) * (1 + zs * n_gl + d)], {"tp": lax.rem(k + (1, n_tp - 1)[d], n_tp)},
        )

    def x_from(d):
        return lax.rem(k + (n_tp - 1, 1)[d], n_tp)

    def x_both(zs, q):
        x_move(0, k, zs, q).start()
        x_move(1, k, zs, q).start()

    def x_pass(d, slot, zs, q):
        return remote(
            wf.at[slot, pair(zs), rows(q)], wf.at[slot, pair(zs), rows(q)], r_send, x_recv.at[0],
            {"tp": lax.rem(k + (1, n_tp - 1)[d], n_tp)},
        )

    def relay(zs, q):
        if n_gl == 1:
            x_move(0, x_from(0), zs, q).wait_recv()
            x_pass(0, x_from(0), zs, q).start()
            return
        for d in range(2):

            @pl.when(q == d)
            def _():
                x_move(d, x_from(d), zs, d).wait_recv()
                x_pass(d, x_from(d), zs, d).start()

    def chips_at(level):
        if level == 0:
            return [z]
        if level == top:
            return [chip(top)]
        return [chip(-level), chip(level)]

    def arrive(level):
        for zs in chips_at(level):
            here = wf.at[k, pair(zs), rows(p)]
            remote(here, here, fz_send, wz_recv.at[zs], sibling).wait_recv()
            if n_gl == 2:
                to_pair(zs, p).start()
            x_both(zs, p)

    def other_half(level):
        if n_gl == 2:
            for zs in chips_at(level):
                to_pair(zs, 1 - p).wait_recv()
                x_both(zs, 1 - p)

    def forward(level, first, last):
        def one(j, carry):
            for prim in (True, False):

                @pl.when(j <= length[prim] - level)
                def _():
                    if level > 0:
                        z_wait(prim, level, j)
                    z_move(prim, level, j).start()

            return carry

        if first < last:
            lax.fori_loop(first, last, one, 0)

    def deliver(level):
        for prim in (True, False):
            if level < length[prim]:
                if level > 0:
                    z_wait(prim, level, 1)
                for c2 in range(2):
                    z_final(prim, level, c2).start()

    def part(ref, slot, q):
        return ref.at[slot, pl.ds(q * sub, sub)]

    def token(slot, q):
        return ct.at[slot] if q == 2 else part(xt, slot, q)

    def mine(q):
        return cq if q == 2 else xq.at[pl.ds(q * sub, sub)]

    t_recv = {True: tp_recv, False: ts_recv}

    def t_move(prim, h, q):
        step = steps[prim]
        slot = 2 * chip(-step * h) + core
        return remote(
            mine(q) if h == 0 else token(slot, q), token(slot, q), t_send.at[q // 2],
            t_recv[prim].at[h, q], {"z": chip(step)},
        )

    def t_wait(prim, h, q):
        here = token(2 * chip(-steps[prim] * h) + core, q)
        remote(here, here, t_send.at[q // 2], t_recv[prim].at[h - 1, q], sibling).wait_recv()

    def t_sibling(h, zs, q):
        slot = 2 * zs + core
        group = {0: 0, top - 1: 1}.get(h, 2)
        return remote(
            mine(q) if h == 0 else token(slot, q), token(slot, q), tb_send.at[q // 2], tb_recv.at[group, q // 2], sibling
        )

    def t_own(q):
        return pltpu.make_async_copy(mine(q), token(me, q), l_sem.at[1 + q])

    def tokens_out():
        for q in (2, 0, 1):
            for prim in (True, False):
                if length[prim] > 0:
                    t_move(prim, 0, q).start()
        for q in (2, 0, 1):
            t_sibling(0, z, q).start()
            t_own(q).start()

    def tokens_at(h):
        for q in (2, 0, 1):
            for prim in (True, False):
                if h <= length[prim]:
                    t_wait(prim, h, q)
                    if h < length[prim]:
                        t_move(prim, h, q).start()
                    t_sibling(h, chip(-steps[prim] * h), q).start()

    def own_block():
        return pltpu.make_async_copy(w.at[me], wf.at[k, me], l_sem.at[0])

    def sib_block(sender):
        return remote(w.at[2 * z + 1 - core], wf.at[k, sender], ws_send, ws_recv, sibling)

    relays = [(0, turn) for turn in range(n_gl)] + [
        (level, turn) for level in range(1, top + 1) for turn in range(n_gl)
    ]

    def pass_on(level, turn):
        while relays and relays[0] <= (level, turn):
            here, which = relays.pop(0)
            for zs in chips_at(here):
                relay(zs, which if here == 0 else lax.rem(p + which, n_gl))

    mixed_from = max(top - 2, 1)

    def weights_at(level):
        arrive(level)
        deliver(level)
        early = level <= mixed_from - 2
        if early and level > 1:
            pass_on(level - 1, 0)
        forward(level, 2, min(4, top - level + 1))
        if level <= mixed_from:
            other_half(level)
        if early:
            pass_on(level - 1, 1)
        forward(level, 4, top - level + 1)
        if level == mixed_from - 1:
            pass_on(level - 1, 0)
        if level == mixed_from:
            pass_on(level - 2, 1)

    after = {1: (top - 3, 0), 2: (top - 2, 0), 3: (top - 2, 1), 4: (top - 1, 1), 5: (top, 1)}
    due = list(range(mixed_from + 1, top + 1))

    def tokens_and_more(h, ready):
        tokens_at(h)
        if due and due[0] <= ready and h > 1:
            other_half(due.pop(0))
        if ready >= after.get(h, (top, 1))[0]:
            pass_on(*after.get(h, (-1, 0)))

    prepare(0)
    own_block().start()
    sib_block(me).start()
    deliver(0)
    forward(0, 2, 3)
    prepare(1)
    forward(0, 3, top + 1)
    own_block().wait()
    sib_block(me + 1 - 2 * core).wait_recv()
    for q in range(n_gl):
        x_both(z, q)
    prepare(2)
    h = 0
    for level in range(1, top + 1):
        if level == mixed_from:
            tokens_out()
        weights_at(level)
        if level >= mixed_from:
            h += 1
            tokens_and_more(h, level)

    def settle_weights():
        while due:
            other_half(due.pop(0))
        pass_on(top, 1)
        both = wf.at[pl.ds(0, 2)]
        remote(both, both, x_send, x_recv.at[0], sibling).wait_recv()
        for q in range(3):
            t_own(q).wait()

    def settle_tokens(group, count):
        for i, ref in enumerate((xt, ct)):
            here = ref.at[pl.ds(0, count)]
            remote(here, here, tb_send.at[i], tb_recv.at[group, i], sibling).wait_recv()

    started = h >= top
    for h in range(h + 1, top):
        tokens_and_more(h, top)
        if h == top - 2 and not relays and not due:
            settle_weights()
            settle_tokens(0, 1)
            first()
            started = True
    if not started or h >= top:
        settle_weights()
        settle_tokens(0, 1)
        first()
    settle_tokens(1, 2)
    second()
    if h < top:
        tokens_and_more(top, top)
    third()
    settle_tokens(2, n_z - 3)

    def drain():
        sib_block(me).wait_send()

        def sent(ref, sem):
            remote(ref, ref, sem, sem, sibling).wait_send()

        sent(wf.at[pl.ds(0, 2)], x_send)
        sent(wf.at[0], r_send)
        if n_gl == 2:
            sent(wf.at[0, pl.ds(0, n_z - 1)], y_send)
        sent(wf.at[0, pl.ds(0, 2 * (n_z - 1) // n_gl)], fz_send)
        sent(tbp, zp_send)
        if top > 2:
            sent(tbs, zs_send)
        for i, ref in enumerate((xt, ct)):
            sent(ref.at[pl.ds(0, n_z - 1)], t_send.at[i])
            sent(ref.at[pl.ds(0, n_z)], tb_send.at[i])

    return drain


def bring_scratch(n_z, n_tp, n_gl, w, xq, cq):
    top, n_fs = n_z // 2, 2 * n_z
    dma = pltpu.SemaphoreType.DMA
    prim, sec = top * (top + 1) // 2, top * (top - 1) // 2
    half = w[1] // n_gl
    return [
        pltpu.VMEM((n_tp, n_fs) + w[1:], bf16),
        pltpu.VMEM((n_fs,) + xq, bf16),
        pltpu.VMEM((n_fs,) + cq, f32),
        pltpu.VMEM((prim - top, 2, half, w[2]), bf16),
        pltpu.VMEM((max(sec - top + 1, 1), 2, half, w[2]), bf16),
        dma(()), dma((prim - top,)), dma(()), dma((max(sec - top + 1, 1),)),
        dma(()), dma((n_z,)), dma(()), dma((n_z,)), dma(()), dma((1 + n_z * n_gl,)), dma(()),
        dma((2,)), dma((top, 3)), dma((top - 1, 3)), dma((2,)), dma((3, 2)),
        dma((4,)), dma(()), dma(()),
    ]


def whole_kernel(
    n_z, n_tp, n_gl, n_bring, prompt, routes, weight, gain, gate, up, down,
    gate_out, up_out, down_out, mixed_out, w, xq, cq, g_in, u_in, d_in, in_sem, x_sem, out_sem, *scratch
):
    z, core, k, p = (lax.axis_index(a) for a in ("z", "core", "tp", "gl"))
    barrier = pltpu.get_barrier_semaphore()
    peers = [{"z": lax.rem(z + d, n_z), "core": c} for d in (1, n_z - 1) for c in range(2)]
    peers += [{"core": 1 - core}] + [{"tp": lax.rem(k + step, n_tp)} for step in range(1, n_tp)]
    if n_gl == 2:
        peers += [{"gl": 1 - p}]
    slots = g_in.shape[0]
    gate_rows, ffq = gate_out.shape[1:]
    share, cols = down_out.shape[0], w.shape[2]
    tok, width = xq.shape

    def fetch(n):
        off = ((n + 1) // 2) * (2 * (n % 2) - 1)
        rows = pl.ds(2 * lax.rem(z + off + n_z, n_z), 2)
        slot = lax.rem(n, slots)
        return [
            pltpu.make_async_copy(src.at[rows], dst.at[slot], in_sem.at[slot, i])
            for i, (src, dst) in enumerate(((gate, g_in), (up, u_in), (down, d_in)))
        ]

    def fetch_prompt():
        return pltpu.make_async_copy(prompt.at[pl.ds(pl.multiple_of(k * tok, tok), tok)], xq, x_sem)

    for n in range(slots):
        for copy in fetch(n):
            copy.start()
    fetch_prompt().start()
    for peer in peers:
        pl.semaphore_signal(barrier, inc=1, device_id=peer, device_id_type=MESH)
    square = lax.broadcasted_iota(jnp.int32, (gate_rows, gate_rows), 0) == lax.broadcasted_iota(
        jnp.int32, (gate_rows, gate_rows), 1
    )
    column = jnp.sum(jnp.where(square, gain[...], 0.0), axis=1, keepdims=True)

    def convert(n, carry):
        off = ((n + 1) // 2) * (2 * (n % 2) - 1)
        first = 2 * lax.rem(z + off + n_z, n_z)
        slot = lax.rem(n, slots)
        for copy in fetch(n):
            copy.wait()
        for e in range(2):
            w[first + e, :gate_rows, :ffq] = (column * g_in[slot, e]).astype(bf16)
            w[first + e, :gate_rows, ffq:] = (column * u_in[slot, e]).astype(bf16)
            w[first + e, gate_rows:, :] = d_in[slot, e].astype(bf16)

        @pl.when(n + slots < n_z)
        def _():
            for copy in fetch(n + slots):
                copy.start()

        return carry

    def normalize(r, carry):
        rows = pl.ds(pl.multiple_of(r * 16, 16), 16)
        v = xq[rows, :].astype(f32)
        xq[rows, :] = (v * lax.rsqrt(jnp.mean(v * v, axis=-1, keepdims=True) + EPS)).astype(bf16)
        return carry

    def part_of(ref):
        mine = ref[:, :tok]
        for t in range(1, n_tp):
            mine = jnp.where(k == t, ref[:, t * tok : (t + 1) * tok], mine)
        return mine

    def prepare(stage):
        early = min(5, n_z)
        if stage == 0:
            lax.fori_loop(0, early, convert, 0)
            pl.semaphore_wait(barrier, len(peers))
        if stage == 1:
            lax.fori_loop(early, n_z, convert, 0)
        if stage == 2:
            fetch_prompt().wait()
            lax.fori_loop(0, tok // 16, normalize, 0)
            chosen, amount = part_of(routes), part_of(weight)
            index = lax.broadcasted_iota(jnp.int32, (cq.shape[0], tok), 0)
            total = jnp.zeros((cq.shape[0], tok), f32)
            for j in range(chosen.shape[0]):
                total += jnp.where(index == chosen[j : j + 1, :], amount[j : j + 1, :], 0.0)
            cq[...] = jnp.zeros_like(cq)
            cq[:, :tok] = total

    for_bring, for_apply = scratch[:n_bring], scratch[n_bring:]
    wf, xt, ct = for_bring[:3]
    outs = [
        pltpu.make_async_copy(wf.at[k, :, :gate_rows, :ffq], gate_out, out_sem.at[0]),
        pltpu.make_async_copy(wf.at[k, :, :gate_rows, ffq:], up_out, out_sem.at[1]),
    ]
    for t in range(n_tp):
        outs.append(
            pltpu.make_async_copy(
                wf.at[t, pl.ds(k * share, share), gate_rows:, :],
                down_out.at[:, :, t * cols : (t + 1) * cols],
                out_sem.at[2 + t],
            )
        )
    first, second, third, rest = apply_and_return(n_z, n_tp, wf, xt, ct, mixed_out, *for_apply)

    def weights_ready():
        for copy in outs:
            copy.start()
        first()

    drain = bring(n_z, n_tp, n_gl, prepare, weights_ready, second, third, w, xq, cq, *for_bring)

    def finish():
        for copy in outs:
            copy.wait()
        drain()

    rest(finish)


def hand_over(*refs):
    n = (len(refs) - 2) // 3
    srcs, outs, bufs = refs[:n], refs[n : 2 * n], refs[2 * n : 3 * n]
    in_sem, out_sem = refs[3 * n :]
    reads, writes = [], []
    for i, (src, out, buf) in enumerate(zip(srcs, outs, bufs)):
        half = src.shape[0] // 2
        for j in range(2):
            rows = pl.ds(j * half, half)
            reads.append(pltpu.make_async_copy(src.at[rows], buf.at[rows], in_sem.at[i, j]))
            writes.append(pltpu.make_async_copy(buf.at[rows], out.at[rows], out_sem.at[i, j]))
    for copy in reads:
        copy.start()
    for read, write in zip(reads, writes):
        read.wait()
        write.start()
    for copy in writes:
        copy.wait()


def shards(prompt, routes, route_weight, norm_gain, gate_train, up_train, down_train):
    n_tp, n_z, n_gl = lax.axis_size("tp"), lax.axis_size("z"), lax.axis_size("gl")
    n_fs = 2 * n_z
    experts, gate_rows, ffq = gate_train.shape
    down_rows, cols = down_train.shape[1:]
    tok, d = prompt.shape[0] // n_tp, prompt.shape[1]
    lanes = -(-tok // 128) * 128
    share = n_fs // n_tp
    slots = 3
    w_shape = (experts, gate_rows + down_rows, cols)
    x_shape, c_shape = (tok, d), (experts, lanes)
    vmem = pl.BlockSpec(memory_space=pltpu.VMEM)
    hbm = pl.BlockSpec(memory_space=pl.ANY)
    for_bring = bring_scratch(n_z, n_tp, n_gl, w_shape, x_shape, c_shape)
    dma = pltpu.SemaphoreType.DMA
    gate_own, up_own, down_own, mixed = pl.pallas_call(
        functools.partial(whole_kernel, n_z, n_tp, n_gl, len(for_bring)),
        out_shape=(
            jax.ShapeDtypeStruct((n_fs, gate_rows, ffq), bf16),
            jax.ShapeDtypeStruct((n_fs, gate_rows, ffq), bf16),
            jax.ShapeDtypeStruct((share, down_rows, n_tp * cols), bf16),
            jax.ShapeDtypeStruct((tok * n_tp, cols), bf16),
        ),
        in_specs=[hbm] + [vmem] * 3 + [hbm] * 3,
        out_specs=(hbm, hbm, hbm, vmem),
        scratch_shapes=[
            pltpu.VMEM(w_shape, bf16),
            pltpu.VMEM(x_shape, bf16),
            pltpu.VMEM(c_shape, f32),
            pltpu.VMEM((slots, 2, gate_rows, ffq), f32),
            pltpu.VMEM((slots, 2, gate_rows, ffq), f32),
            pltpu.VMEM((slots, 2, down_rows, cols), f32),
            dma((slots, 3)),
            dma(()),
            dma((2 + n_tp,)),
        ]
        + for_bring
        + apply_scratch(n_z, n_tp, n_fs, tok, d),
        compiler_params=pltpu.CompilerParams(
            collective_id=0, has_side_effects=True, vmem_limit_bytes=67043328
        ),
    )(prompt, routes.T, route_weight.T, norm_gain[None, :], gate_train, up_train, down_train)
    results = (gate_own, up_own, down_own, mixed)
    gate_own, up_own, down_own, mixed = pl.pallas_call(
        hand_over,
        out_shape=tuple(jax.ShapeDtypeStruct(a.shape, a.dtype) for a in results),
        in_specs=[hbm] * 4,
        out_specs=[hbm] * 4,
        scratch_shapes=[pltpu.VMEM(a.shape, a.dtype) for a in results] + [dma((4, 2)), dma((4, 2))],
        compiler_params=pltpu.CompilerParams(vmem_limit_bytes=67043328),
    )(*results)
    return (
        gate_own.reshape(1, d, ffq),
        up_own.reshape(1, d, ffq),
        down_own.reshape(1, share * down_rows, n_tp * cols),
        mixed,
    )


def solution(mesh):
    groups, n_tp = mesh.shape["grp"], mesh.shape["tp"]
    chips = mesh.shape["fs"] // 2
    pair = 2 if groups % 2 == 0 else 1
    finer = Mesh(
        mesh.devices.reshape(groups // pair, pair, chips, 2, n_tp),
        ("gh", "gl", "z", "core", "tp"),
    )
    return jax.shard_map(
        shards,
        mesh=finer,
        in_specs=(P(ROWS), P(ROWS), P(ROWS), P(FS), P(None, FS, "tp"), P(None, FS, "tp"), P(None, FS, "tp")),
        out_specs=(P(ROWS, None, "tp"), P(ROWS, None, "tp"), P(ROWS, "tp", None), P(ROWS, "tp")),
        check_vma=False,
    )
```

time: 278 us -> 245 us (0.88)
  Pallas kernels: 261 us -> 244 us
  other arithmetic: 7.41 us -> 0 us
  local copies, waits for them, and re-layouts: 7.4 us -> 0 us
    pallas_call x1, Pallas kernels: 261 us -> 241 us  [shards(): pl.pallas_call(functools.partial(whole_kernel, n_z, n_tp, n_gl, len(for_b...]
    unnamed x16 -> x0, local copies, waits for them, and re-layouts: 5.12 us -> none
    convert_element_type x3 -> x0, other arithmetic: 4.25 us -> none  [the longest x1 1.87 us: shards(): (x * lax.rsqrt(jnp.mean(x * x, axis=-1, keepdims=True) + EPS)).astype(bf16)]
    pallas_call x0 -> x1, Pallas kernels: none -> 2.96 us  [shards(): pl.pallas_call(hand_over, out_shape=tuple((jax.ShapeDtypeStruct(a.shape,...]
where the time goes in v2:
time: 245 us
  Pallas kernels  244 us (100%)
    pallas_call x1, Pallas kernels, shards(): pl.pallas_call(functools.partial(whole_kernel, n_z, n_tp, n_gl, len(for_b...  241 us

profile of v2, /device:TPU:40, one launch (start us, length us, event | category | flops | bytes accessed | tf_op | source)
XLA Modules:
  0.0 245.0 jit_solution(7791324749981659982)
XLA Ops:
  0.6 241.2 %shard_map.102 = (bf16[32,64,256]{2,1,0:T(8,128)(2,1)}, bf16[32,64,256]{2,1,0:T(8,128)(2,1)}, bf16[8,32,2048]{2,1,0:T(8,128)(2,1)}, bf16[384,512]{1,0:T(8,128)(2,1)}) custom-call(bf16[384,2048]{1,0:T(8,128)(2,1)} %prompt.1, s32[4,384]{1,0:T(4,128)} %bitcast.6, f32[4,384]{1,0:T(4,128)} %bitcast.7, f32[1,64]{1,0:T(1,128)} %bitcast.8, f32[32,64,256]{2,1,0:T(8,128)} %gate.1, ...), custom_call_target="tpu_custom_call" | custom-call | tf_op jit(solution)/shard_map/pallas_call | solution.py:709
  241.8 3.0 %shard_map.103 = (bf16[32,64,256]{2,1,0:T(8,128)(2,1)}, bf16[32,64,256]{2,1,0:T(8,128)(2,1)}, bf16[8,32,2048]{2,1,0:T(8,128)(2,1)}, bf16[384,512]{1,0:T(8,128)(2,1)}) custom-call(bf16[32,64,256]{2,1,0:T(8,128)(2,1)} %get-tuple-element.12.refs_0_, bf16[32,64,256]{2,1,0:T(8,128)(2,1)} %get-tuple-element.13.refs_1_, ...), custom_call_target="tpu_custom_call" | custom-call | tf_op jit(solution)/shard_map/pallas_call | solution.py:737

commit v3 on v2

--- a/solution.py
+++ b/solution.py
@@ -44,8 +44,12 @@
         j = steps - i
         return lax.rem(z + j, n_z), lax.rem(z - j + n_z, n_z)
 
-    def inner(some):
-        x = jnp.concatenate([xt[pl.ds(2 * chip, 2)].reshape(2 * tok, width) for chip in some], axis=0)
+    def span(q):
+        return (0, tok) if q is None else (q * sub, sub)
+
+    def inner(some, q=None):
+        at, count = span(q)
+        x = jnp.concatenate([xt[2 * chip + c, at : at + count, :] for chip in some for c in range(2)], axis=0)
         count = x.shape[0]
         for t in range(n_tp):
             gu = jnp.dot(x, wf[t, :, :gate_rows, :].reshape(width, cols), preferred_element_type=f32)
@@ -53,24 +57,26 @@
             u = jnp.clip(gu[:, ffq:], -LIMIT, LIMIT)
             hid[:count, t * ffq : (t + 1) * ffq] = ((u + 1.0) * g * jax.nn.sigmoid(ALPHA * g)).astype(bf16)
 
-    def outer(some, places):
-        count = 2 * tok * len(some)
+    def outer(some, places, q=None):
+        at, count = span(q)
+        total = 2 * count * len(some)
         eye = lax.broadcasted_iota(jnp.int32, (tok, ct.shape[2]), 0) == lax.broadcasted_iota(
             jnp.int32, (tok, ct.shape[2]), 1
         )
+        own = lax.broadcasted_iota(jnp.int32, ct.shape[1:], 0) == 2 * z + core
         scales = []
         for chip in some:
             for c in range(2):
-                row = ct[2 * chip + c, pl.ds(2 * z + core, 1), :]
-                scales.append(jnp.sum(jnp.where(eye, row, 0.0), axis=1, keepdims=True))
+                row = jnp.sum(jnp.where(own, ct[2 * chip + c].astype(f32), 0.0), axis=0, keepdims=True)
+                scales.append(jnp.sum(jnp.where(eye, row, 0.0), axis=1, keepdims=True)[at : at + count])
         scale = jnp.concatenate(scales, axis=0)
         for t in range(n_tp):
             down = wf[t, :, gate_rows:, :].reshape(wf.shape[1] * down_rows, cols)
-            part = (scale * jnp.dot(hid[:count, :], down, preferred_element_type=f32)).astype(bf16)
+            part = (scale * jnp.dot(hid[:total, :], down, preferred_element_type=f32)).astype(bf16)
             for n, (i, w) in enumerate(places):
                 for c in range(2):
-                    at = (2 * n + c) * tok
-                    cb[i, w, c, :, t * cols : (t + 1) * cols] = part[at : at + tok]
+                    here = (2 * n + c) * count
+                    cb[i, w, c, at : at + count, t * cols : (t + 1) * cols] = part[here : here + count]
 
     def b_slot(i, w):
         return steps * w if isinstance(i, int) and i == 0 else i
@@ -129,13 +135,14 @@
         for w in range(2):
             to_sibling(i, w).start()
 
-    def body(i, carry):
-        sib_in(i)
-        combine_s(i, 0)
+    def begin(i):
+        @pl.when(i > 1)
+        def _():
+            sib_in(i)
+            combine_s(i, 0)
 
         @pl.when(i == 1)
         def _():
-            combine_s(i, 1)
             to_sibling(0, 0).wait_recv()
 
         combine_p(i - 1, 0)
@@ -144,16 +151,24 @@
         def _():
             combine_p(i - 1, 1)
 
-        inner(chips(i + 1))
-
+    def end(i):
         @pl.when(i > 1)
         def _():
             combine_s(i, 1)
             combine_p(i - 1, 1)
 
-        outer(chips(i + 1), [(i + 1, 0), (i + 1, 1)])
-        sib_out(i + 1)
+    def body(i, carry):
+        begin(i)
+        inner(chips(i + 2))
+        end(i)
+        outer(chips(i + 2), [(i + 2, 0), (i + 2, 1)])
+        sib_out(i + 2)
         return carry
+
+    def ahead_of_near():
+        inner(chips(2))
+        outer(chips(2), [(2, 0), (2, 1)])
+        sib_out(2)
 
     def one_chip(chip, w):
         inner([chip])
@@ -171,22 +186,37 @@
     def first():
         one_chip(z, 1)
 
-    def second():
-        inner(chips(1))
-
-    def third():
-        outer(chips(1), [(1, 0), (1, 1)])
-        sib_out(1)
+    def near_sibling(w, q):
+        rows = pl.ds(q * sub, sub)
+        return remote(
+            cb.at[1, w, 1 - core, rows], sib.at[1, w, rows], b_send, b_recv.at[1 + q * steps], sibling
+        )
+
+    def second(q):
+        inner(chips(1), q)
+        outer(chips(1), [(1, 0), (1, 1)], q)
+        for w in range(2):
+            near_sibling(w, q).start()
+
+    def third(q):
+        here = sib.at[1, :, pl.ds(q * sub, sub)]
+        remote(here, here, b_send, b_recv.at[1 + q * steps], sibling).wait_recv()
+        combine_s(1, q)
 
     def rest(drain_bring):
         one_chip(lax.rem(z + steps, n_z), 0)
-        lax.fori_loop(1, steps - 1, body, 0)
+        lax.fori_loop(1, max(steps - 2, 1), body, 0)
         last = steps - 1
-        sib_in(last)
+        if last > 1:
+            begin(last - 1)
+            end(last - 1)
         if last == 1:
             to_sibling(0, 0).wait_recv()
+        else:
+            sib_in(last)
         for q in range(2):
-            combine_s(last, q)
+            if last > 1:
+                combine_s(last, q)
             combine_p(last - 1, q)
         for q in range(2):
             combine_p(last, q)
@@ -213,7 +243,7 @@
         sent(peers, f_send)
         remote(peers, peers, f_send, f_recv, sibling).wait_recv()
 
-    return first, second, third, rest
+    return first, ahead_of_near, second, third, rest
 
 
 def apply_scratch(n_z, n_tp, n_fs, tok, width):
@@ -226,12 +256,12 @@
         pltpu.VMEM((steps + 1, tok, width), bf16),
         pltpu.VMEM((steps + 1, tok, width), bf16),
         pltpu.VMEM((n_tp, tok, width // n_tp), bf16),
-        dma(()), dma((steps, 2)), dma(()), dma((steps - 1, 2)), dma(()), dma((steps + 1,)), dma(()), dma(()),
+        dma(()), dma((steps, 2)), dma(()), dma((steps - 1, 2)), dma(()), dma((steps + 2,)), dma(()), dma(()),
     ]
 
 
 def bring(
-    n_z, n_tp, n_gl, prepare, first, second, third, w, xq, cq, wf, xt, ct, tbp, tbs,
+    n_z, n_tp, n_gl, prepare, first, ahead_of_near, second, third, w, xq, cq, wf, xt, ct, tbp, tbs,
     zp_send, zp_recv, zs_send, zs_recv, fz_send, wz_recv, y_send, y_recv, x_send, x_recv, r_send,
     t_send, tp_recv, ts_recv, tb_send, tb_recv, l_sem, ws_send, ws_recv,
 ):
@@ -390,7 +420,7 @@
 
     def t_sibling(h, zs, q):
         slot = 2 * zs + core
-        group = {0: 0, top - 1: 1}.get(h, 2)
+        group = 0 if h == 0 else 4 if h == top - 2 else 3 if h != top - 1 else 2 if q == 1 else 1
         return remote(
             mine(q) if h == 0 else token(slot, q), token(slot, q), tb_send.at[q // 2], tb_recv.at[group, q // 2], sibling
         )
@@ -407,8 +437,8 @@
             t_sibling(0, z, q).start()
             t_own(q).start()
 
-    def tokens_at(h):
-        for q in (2, 0, 1):
+    def tokens_at(h, parts=(2, 0, 1)):
+        for q in parts:
             for prim in (True, False):
                 if h <= length[prim]:
                     t_wait(prim, h, q)
@@ -491,29 +521,46 @@
         for q in range(3):
             t_own(q).wait()
 
-    def settle_tokens(group, count):
-        for i, ref in enumerate((xt, ct)):
-            here = ref.at[pl.ds(0, count)]
+    def settle_tokens(group, *refs):
+        for i, here in enumerate(refs):
             remote(here, here, tb_send.at[i], tb_recv.at[group, i], sibling).wait_recv()
 
-    started = h >= top
-    for h in range(h + 1, top):
+    def own_tokens():
+        settle_weights()
+        settle_tokens(0, xt.at[pl.ds(0, 1)], ct.at[pl.ds(0, 1)])
+        first()
+
+    def near_tokens(q):
+        here = xt.at[pl.ds(0, 2), pl.ds(0, sub)]
+        settle_tokens(1 + q, *((here, ct.at[pl.ds(0, 2)])[: 2 - q]))
+        second(q)
+
+    started = False
+    while h + 1 < top - 1:
+        h += 1
         tokens_and_more(h, top)
         if h == top - 2 and not relays and not due:
-            settle_weights()
-            settle_tokens(0, 1)
-            first()
+            own_tokens()
             started = True
-    if not started or h >= top:
-        settle_weights()
-        settle_tokens(0, 1)
-        first()
-    settle_tokens(1, 2)
-    second()
+    if not started:
+        own_tokens()
+    if h < top - 1:
+        tokens_at(top - 1, (2, 0))
+    if top > 2:
+        settle_tokens(4, xt.at[pl.ds(0, 2)], ct.at[pl.ds(0, 2)])
+        ahead_of_near()
+    if h < top - 1:
+        tokens_at(top - 1, (1,))
     if h < top:
-        tokens_and_more(top, top)
-    third()
-    settle_tokens(2, n_z - 3)
+        tokens_at(top, (2, 0))
+    near_tokens(0)
+    near_tokens(1)
+    third(0)
+    if h < top:
+        tokens_at(top, (1,))
+    third(1)
+    rest = pl.ds(0, n_z - (5 if top > 2 else 3))
+    settle_tokens(3, xt.at[rest], ct.at[rest])
 
     def drain():
         sib_block(me).wait_send()
@@ -544,12 +591,12 @@
     return [
         pltpu.VMEM((n_tp, n_fs) + w[1:], bf16),
         pltpu.VMEM((n_fs,) + xq, bf16),
-        pltpu.VMEM((n_fs,) + cq, f32),
+        pltpu.VMEM((n_fs,) + cq, bf16),
         pltpu.VMEM((prim - top, 2, half, w[2]), bf16),
         pltpu.VMEM((max(sec - top + 1, 1), 2, half, w[2]), bf16),
         dma(()), dma((prim - top,)), dma(()), dma((max(sec - top + 1, 1),)),
         dma(()), dma((n_z,)), dma(()), dma((n_z,)), dma(()), dma((1 + n_z * n_gl,)), dma(()),
-        dma((2,)), dma((top, 3)), dma((top - 1, 3)), dma((2,)), dma((3, 2)),
+        dma((2,)), dma((top, 3)), dma((top - 1, 3)), dma((2,)), dma((5, 2)),
         dma((4,)), dma(()), dma(()),
     ]
 
@@ -638,7 +685,7 @@
             for j in range(chosen.shape[0]):
                 total += jnp.where(index == chosen[j : j + 1, :], amount[j : j + 1, :], 0.0)
             cq[...] = jnp.zeros_like(cq)
-            cq[:, :tok] = total
+            cq[:, :tok] = total.astype(bf16)
 
     for_bring, for_apply = scratch[:n_bring], scratch[n_bring:]
     wf, xt, ct = for_bring[:3]
@@ -654,14 +701,14 @@
                 out_sem.at[2 + t],
             )
         )
-    first, second, third, rest = apply_and_return(n_z, n_tp, wf, xt, ct, mixed_out, *for_apply)
+    first, ahead_of_near, second, third, rest = apply_and_return(n_z, n_tp, wf, xt, ct, mixed_out, *for_apply)
 
     def weights_ready():
         for copy in outs:
             copy.start()
         first()
 
-    drain = bring(n_z, n_tp, n_gl, prepare, weights_ready, second, third, w, xq, cq, *for_bring)
+    drain = bring(n_z, n_tp, n_gl, prepare, weights_ready, ahead_of_near, second, third, w, xq, cq, *for_bring)
 
     def finish():
         for copy in outs:
@@ -719,7 +766,7 @@
         scratch_shapes=[
             pltpu.VMEM(w_shape, bf16),
             pltpu.VMEM(x_shape, bf16),
-            pltpu.VMEM(c_shape, f32),
+            pltpu.VMEM(c_shape, bf16),
             pltpu.VMEM((slots, 2, gate_rows, ffq), f32),
             pltpu.VMEM((slots, 2, gate_rows, ffq), f32),
             pltpu.VMEM((slots, 2, down_rows, cols), f32),

time: 245 us -> 245 us (level)
  no operation moved by 1% of the time
where the time goes in v3:
time: 245 us; the launch traced here: 243 us
  Pallas kernels  242 us (99%)
    pallas_call x1, Pallas kernels, shards(): pl.pallas_call(functools.partial(whole_kernel, n_z, n_tp, n_gl, len(for_b...  239 us

profile of v3, /device:TPU:40, one launch (start us, length us, event | category | flops | bytes accessed | tf_op | source)
XLA Modules:
  0.0 243.2 jit_solution(5301913675554880076)
XLA Ops:
  0.6 239.4 %shard_map.102 = (bf16[32,64,256]{2,1,0:T(8,128)(2,1)}, bf16[32,64,256]{2,1,0:T(8,128)(2,1)}, bf16[8,32,2048]{2,1,0:T(8,128)(2,1)}, bf16[384,512]{1,0:T(8,128)(2,1)}) custom-call(bf16[384,2048]{1,0:T(8,128)(2,1)} %prompt.1, s32[4,384]{1,0:T(4,128)} %bitcast.6, f32[4,384]{1,0:T(4,128)} %bitcast.7, f32[1,64]{1,0:T(1,128)} %bitcast.8, f32[32,64,256]{2,1,0:T(8,128)} %gate.1, ...), custom_call_target="tpu_custom_call" | custom-call | tf_op jit(solution)/shard_map/pallas_call | solution.py:756
  240.1 3.0 %shard_map.103 = (bf16[32,64,256]{2,1,0:T(8,128)(2,1)}, bf16[32,64,256]{2,1,0:T(8,128)(2,1)}, bf16[8,32,2048]{2,1,0:T(8,128)(2,1)}, bf16[384,512]{1,0:T(8,128)(2,1)}) custom-call(bf16[32,64,256]{2,1,0:T(8,128)(2,1)} %get-tuple-element.12.refs_0_, bf16[32,64,256]{2,1,0:T(8,128)(2,1)} %get-tuple-element.13.refs_1_, ...), custom_call_target="tpu_custom_call" | custom-call | tf_op jit(solution)/shard_map/pallas_call | solution.py:784
